TPU v7x, 512 devices: a 4x2x32 block of a 4x8x32 slice. The times are simulated.
512 devices in a mesh: grp: 2 (over y), ep: 64 (over z, core), tp: 4 (over x).
Axes of the slice: x: 4, y: 2, z: 32, core: 2. Of those that a mesh axis runs over, the one named last changes fastest.
The devices are a block of a 4x8x32 slice.
Arguments:
- tokens: bfloat16 [49152, 2048], P(('grp', 'ep'), 'tp'), parts along dimension 0
- group_choice: int32 [49152], P(('grp', 'ep')), parts along dimension 0, may hold values from 0 to 7, as said below
- expert_choice: int32 [49152, 2], P(('grp', 'ep')), parts along dimension 0, may hold values from 0 to 7, as said below
- group_weight: float32 [49152], P(('grp', 'ep')), parts along dimension 0, may hold values from 0.3 to 1
- expert_weight: float32 [49152, 2], P(('grp', 'ep')), parts along dimension 0, may hold values from 0.1 to 1
- norm_gain: float32 [2048], replicated, may hold values from 0.1 to 1.9
- w_gate: bfloat16 [64, 2048, 1024], P('ep', None, 'tp'), may hold values from -0.125 to 0.125
- w_up: bfloat16 [64, 2048, 1024], P('ep', None, 'tp'), may hold values from -0.125 to 0.125
- w_down: bfloat16 [64, 1024, 2048], P('ep', None, 'tp'), may hold values from -0.1875 to 0.1875
Outputs:
- moe_out: bfloat16 [49152, 2048], P(('grp', 'ep'), 'tp'), parts along dimension 0
There are 2 independent parts, one for each index of `grp`. A program takes and returns all parts, laid end to end along the dimension named above; an argument that names none is the same for every part. Nothing has to cross between parts.
Inputs may be any that keep to these rules, and one draw needn't show every extreme that they name: `group_choice`: group of each token, 0 to 7; within each aligned block of 384 tokens (the tokens of one index of ep) every group is chosen by the same number of tokens. `expert_choice`: a token's two entries differ; within each aligned block of 384 tokens no expert (group with entry) is named by more than 18 tokens, and in every block one expert of each group, the same one in all blocks, is named by exactly 18 tokens.
All inputs are finite; a program needn't handle non-finite values.
Results may differ from a plain program's by a relative error of at most 0.0071.
Values may be sent and summed in bfloat16 or wider, within the bound.
A program may use at most 64 MiB of HBM per device.

v0:
```python
import jax
import jax.numpy as jnp
from jax import lax
from jax.sharding import Mesh
from jax.sharding import PartitionSpec as P

GRP_EP = ("grp", "g", "e")
EP = ("g", "e")
GROUP_SIZE = 8


def rank_before(marks):
    return jnp.cumsum(marks, -2) - marks


def body(
    tokens,
    group_choice,
    expert_choice,
    group_weight,
    expert_weight,
    norm_gain,
    w_gate,
    w_up,
    w_down,
):
    rows, width = tokens.shape
    groups = lax.axis_size("g")
    members = lax.axis_size("e")
    per_group = rows // groups
    mean_load = 2 * per_group // members
    capacity = mean_load + min(mean_load // 2, per_group - mean_load)
    model_width = norm_gain.shape[0]
    mixing = group_weight[:, None] * expert_weight / jnp.sum(expert_weight, -1, keepdims=True)
    group_marks = (group_choice[:, None] == jnp.arange(groups, dtype=jnp.int32)).astype(jnp.int32)
    place = group_choice * per_group + jnp.sum(rank_before(group_marks) * group_marks, 1)
    spots = jnp.arange(rows, dtype=jnp.int32)
    sort = spots[:, None] == place[None, :]
    values = tokens.astype(jnp.float32)
    squares = lax.all_gather(jnp.sum(values * values, -1), "tp", axis=0)
    inv_rms = lax.rsqrt(jnp.sum(squares, 0) / model_width + 1e-06)
    gain = lax.dynamic_slice_in_dim(norm_gain, lax.axis_index("tp") * width, width, 0)
    normed = (values * inv_rms[:, None] * gain[None, :]).astype(jnp.bfloat16)
    by_group = jnp.dot(
        sort.astype(jnp.bfloat16), normed, preferred_element_type=jnp.float32
    ).astype(jnp.bfloat16)
    facts = jnp.concatenate([expert_choice.astype(jnp.float32), mixing], -1)
    facts = jnp.dot(sort.astype(jnp.float32), facts, precision=lax.Precision.HIGHEST)
    landed = lax.all_to_all(
        by_group.reshape(groups, per_group, width), "g", 0, 0, tiled=True
    ).reshape(rows, width)
    facts = lax.all_to_all(facts.reshape(groups, per_group, 4), "g", 0, 0, tiled=True).reshape(
        rows, 4
    )
    chosen = facts[:, :2].astype(jnp.int32).reshape(groups, per_group, 2)
    blocks = jnp.arange(groups, dtype=jnp.int32)[:, None, None]
    kinds = jnp.arange(members, dtype=jnp.int32)
    marks = jnp.sum((chosen[..., None] == kinds).astype(jnp.int32), 2)
    ranks = rank_before(marks)
    seats = jnp.sum(jnp.where(chosen[..., None] == kinds, ranks[:, :, None, :], 0), -1)
    targets = (chosen * groups + blocks) * capacity + seats
    targets = targets.reshape(rows, 2)
    seats_all = members * groups * capacity
    places = jnp.arange(seats_all, dtype=jnp.int32)
    picks = [targets[None, :, k] == places[:, None] for k in range(2)]
    dispatch = (picks[0] | picks[1]).astype(jnp.bfloat16)
    buffer = jnp.dot(dispatch, landed, preferred_element_type=jnp.float32).astype(jnp.bfloat16)
    received = lax.all_to_all(
        buffer.reshape(members, groups * capacity, width), "e", 0, 0, tiled=True
    ).reshape(seats_all, width)
    piece = lax.all_gather(received, "tp", axis=1, tiled=True)
    gate = jnp.dot(piece, w_gate[0], preferred_element_type=jnp.float32)
    up = jnp.dot(piece, w_up[0], preferred_element_type=jnp.float32)
    hidden = (jax.nn.silu(gate) * up).astype(jnp.bfloat16)
    hidden = lax.all_gather(hidden, "tp", axis=1, tiled=True)
    result = jnp.dot(hidden, w_down[0], preferred_element_type=jnp.float32).astype(jnp.bfloat16)
    back = lax.all_to_all(
        result.reshape(members, groups * capacity, width), "e", 0, 0, tiled=True
    ).reshape(seats_all, width)
    mixed = jnp.zeros((rows, width), jnp.float32)
    for k in range(2):
        picker = (targets[:, k : k + 1] == places[None, :]).astype(jnp.bfloat16)
        picked = jnp.dot(picker, back, preferred_element_type=jnp.float32)
        mixed = mixed + facts[:, 2 + k : 3 + k] * picked
    home = lax.all_to_all(
        mixed.astype(jnp.bfloat16).reshape(groups, per_group, width), "g", 0, 0, tiled=True
    ).reshape(rows, width)
    unsort = place[:, None] == spots[None, :]
    return jnp.dot(unsort.astype(jnp.bfloat16), home, preferred_element_type=jnp.float32).astype(
        jnp.bfloat16
    )


def solution(mesh):
    members = GROUP_SIZE
    split = Mesh(
        mesh.devices.reshape(
            mesh.shape["grp"], mesh.shape["ep"] // members, members, mesh.shape["tp"]
        ),
        ("grp", "g", "e", "tp"),
    )
    placed = (
        P(GRP_EP, "tp"),
        P(GRP_EP),
        P(GRP_EP, None),
        P(GRP_EP),
        P(GRP_EP, None),
        P(),
        P(EP, None, "tp"),
        P(EP, None, "tp"),
        P(EP, None, "tp"),
    )
    return jax.shard_map(
        body, mesh=split, in_specs=placed, out_specs=P(GRP_EP, "tp"), check_vma=False
    )
```

profile of v0, /device:TPU:96, one launch (start us, length us, event | category | flops | bytes accessed | tf_op | source)
XLA Modules:
  0.0 404.2 jit_solution(10690738187043938088)
XLA Ops:
  6.6 0.8 convert_element_type.48
  7.3 0.7 fusion.29
  8.0 0.8 reduce-window.6
  9.1 0.8 fusion.28
  9.9 0.7 multiply_add_fusion.1
  10.6 0.7 reduce_sum.57
  11.3 0.7 multiply_divide_fusion
  12.5 0.7 reshape.92
  13.2 42.5 %all-to-all-start = ((f32[8,1,192]{2,1,0:T(1,128)}), f32[8,1,192]{2,1,0:T(1,128)S(1)}, u32[]{:S(2)}, u32[]{:S(2)}) async-start(f32[8,1,192]{2,1,0:T(1,128)} %reshape.92), calls=%async_computation | async-start | bytes 16384 | tf_op jit(solution)/shard_map/all_to_all | solution.py:52
  55.7 1.2 fusion.17
  56.9 11.4 %all-gather.1 = f32[4,1,384]{2,1,0:T(1,128)S(1)} all-gather(f32[1,1,384]{2,1,0:T(1,128)S(1)} %reshape.84), channel_id=2, replica_groups=mesh['grp'=2,'g'=8,'e'=8,'tp'=4] {'tp'}, dimensions={0}, use_global_device_ids=true | all-gather | bytes 7680 | tf_op jit(solution)/shard_map/all_gather | solution.py:40
  68.3 0.8 dynamic_slice.3
  69.1 2.2 convolution_convert_fusion.3
  71.3 6.7 %all-to-all-done = f32[8,1,192]{2,1,0:T(1,128)S(1)} async-done(((f32[8,1,192]{2,1,0:T(1,128)}), f32[8,1,192]{2,1,0:T(1,128)S(1)}, u32[]{:S(2)}, u32[]{:S(2)}) %all-to-all-start) | async-done | bytes 6176 | tf_op jit(solution)/shard_map/all_to_all | solution.py:52
  78.0 15.0 %all-to-all-start.1 = ((bf16[8,48,512]{2,1,0:T(8,128)(2,1)}), bf16[8,48,512]{2,1,0:T(8,128)(2,1)S(1)}, u32[]{:S(2)}, u32[]{:S(2)}) async-start(bf16[8,48,512]{2,1,0:T(8,128)(2,1)} %bitcast.3), calls=%async_computation.1 | async-start | bytes 786432 | tf_op jit(solution)/shard_map/all_to_all | solution.py:49
  93.1 0.6 broadcast.44
  93.7 0.7 reduce.11
  94.8 3.8 reduce-window_subtract_fusion
  98.9 34.6 %all-to-all-done.1 = bf16[8,48,512]{2,1,0:T(8,128)(2,1)S(1)} async-done(((bf16[8,48,512]{2,1,0:T(8,128)(2,1)}), bf16[8,48,512]{2,1,0:T(8,128)(2,1)S(1)}, u32[]{:S(2)}, u32[]{:S(2)}) %all-to-all-start.1) | async-done | bytes 393248 | tf_op jit(solution)/shard_map/all_to_all | solution.py:49
  133.6 0.8 convolution_convert_fusion.1
  134.4 40.5 %all_to_all.25 = bf16[8,144,512]{2,1,0:T(8,128)(2,1)} all-to-all(bf16[8,144,512]{2,1,0:T(8,128)(2,1)S(1)} %bitcast.50), channel_id=1, replica_groups=mesh['grp'=2,'g'=8,'e'=8,'tp'=4] {'e'}, dimensions={0} | all-to-all | bytes 2359296 | tf_op jit(solution)/shard_map/all_to_all | solution.py:68
  175.0 52.6 %all-gather.5.cloned.1.call-done = bf16[1152,2048]{1,0:T(8,128)(2,1)} async-done(((bf16[1152,512]{1,0:T(8,128)(2,1)}), bf16[1152,2048]{1,0:T(8,128)(2,1)}) %all-gather.5.cloned.1.call-update) | async-done | bytes 4718608 | tf_op jit(solution)/shard_map/all_gather | solution.py:71
  227.7 3.9 fusion.11
  231.6 2.4 fusion
  234.0 53.1 %all-gather.7.cloned.1.call-done = bf16[1152,1024]{1,0:T(8,128)(2,1)} async-done(((bf16[1152,256]{1,0:T(8,128)(2,1)}), bf16[1152,1024]{1,0:T(8,128)(2,1)}) %all-gather.7.cloned.1.call-update) | async-done | bytes 2359312 | tf_op jit(solution)/shard_map/all_gather | solution.py:75
  287.2 4.1 %convolution_convert_fusion = bf16[1152,512]{1,0:T(8,128)(2,1)} fusion(bf16[1152,1024]{1,0:T(8,128)(2,1)} %all-gather.7.cloned.1.call-done, bf16[1,1024,512]{2,1,0:T(8,128)(2,1)S(1)} %copy-done), kind=kOutput, calls=%fused_computation | convolution fusion | flops 1208549376 | bytes 4587520 | tf_op jit(solution)/shard_map/dot_general | solution.py:76
  291.2 5.3 %all-to-all-start.3 = ((bf16[8,144,512]{2,1,0:T(8,128)(2,1)}), bf16[8,144,512]{2,1,0:T(8,128)(2,1)S(1)}, u32[]{:S(2)}, u32[]{:S(2)}) async-start(bf16[8,144,512]{2,1,0:T(8,128)(2,1)} %bitcast.10), calls=%async_computation.3 | async-start | bytes 2359296 | tf_op jit(solution)/shard_map/all_to_all | solution.py:77
  296.5 25.9 %all-to-all-done.3 = bf16[8,144,512]{2,1,0:T(8,128)(2,1)S(1)} async-done(((bf16[8,144,512]{2,1,0:T(8,128)(2,1)}), bf16[8,144,512]{2,1,0:T(8,128)(2,1)S(1)}, u32[]{:S(2)}, u32[]{:S(2)}) %all-to-all-start.3) | async-done | bytes 1179680 | tf_op jit(solution)/shard_map/all_to_all | solution.py:77
  322.4 0.7 fusion.7
  323.2 0.7 fusion.8
  323.9 72.3 %all_to_all.26 = bf16[8,48,512]{2,1,0:T(8,128)(2,1)S(1)} all-to-all(bf16[8,48,512]{2,1,0:T(8,128)(2,1)S(1)} %bitcast.52), channel_id=1, replica_groups=mesh['grp'=2,'g'=8,'e'=8,'tp'=4] {'g'}, dimensions={0} | all-to-all | bytes 786432 | tf_op jit(solution)/shard_map/all_to_all | solution.py:85
  396.2 1.2 convolution_convert_fusion.2
  (37 shorter events, 1.8 us)
Async XLA Ops:
  6.5 280.6 %copy-start = (bf16[1,1024,512]{2,1,0:T(8,128)(2,1)S(1)}, bf16[1,1024,512]{2,1,0:T(8,128)(2,1)}, u32[]{:S(2)}) copy-start(bf16[1,1024,512]{2,1,0:T(8,128)(2,1)} %param.17) | copy-start | bytes 3145732
  13.2 64.8 %all-to-all-start = ((f32[8,1,192]{2,1,0:T(1,128)}), f32[8,1,192]{2,1,0:T(1,128)S(1)}, u32[]{:S(2)}, u32[]{:S(2)}) async-start(f32[8,1,192]{2,1,0:T(1,128)} %reshape.92), calls=%async_computation | async-start | bytes 16384 | tf_op jit(solution)/shard_map/all_to_all | solution.py:52
  78.0 55.6 %all-to-all-start.1 = ((bf16[8,48,512]{2,1,0:T(8,128)(2,1)}), bf16[8,48,512]{2,1,0:T(8,128)(2,1)S(1)}, u32[]{:S(2)}, u32[]{:S(2)}) async-start(bf16[8,48,512]{2,1,0:T(8,128)(2,1)} %bitcast.3), calls=%async_computation.1 | async-start | bytes 786432 | tf_op jit(solution)/shard_map/all_to_all | solution.py:49
  92.9 134.7 %all-gather.5.cloned.1.call-start = ((), (), s32[]{:S(2)}) async-start(), calls=%async_computation.5 | async-start | bytes 5898240 | tf_op jit(solution)/shard_map/all_gather | solution.py:71
  174.9 52.8 %copy-start.2 = (bf16[1,2048,256]{2,1,0:T(8,128)(2,1)S(1)}, bf16[1,2048,256]{2,1,0:T(8,128)(2,1)}, u32[]{:S(2)}) copy-start(bf16[1,2048,256]{2,1,0:T(8,128)(2,1)} %param.15) | copy-start | bytes 3145732
  174.9 56.6 %copy-start.3 = (bf16[1,2048,256]{2,1,0:T(8,128)(2,1)S(1)}, bf16[1,2048,256]{2,1,0:T(8,128)(2,1)}, u32[]{:S(2)}) copy-start(bf16[1,2048,256]{2,1,0:T(8,128)(2,1)} %param.16) | copy-start | bytes 3145732
  175.0 112.2 %all-gather.7.cloned.1.call-start = ((), (), s32[]{:S(2)}) async-start(), calls=%async_computation.6 | async-start | bytes 2949120 | tf_op jit(solution)/shard_map/all_gather | solution.py:75
  227.7 3.9 copy-start.1
  291.2 31.2 %all-to-all-start.3 = ((bf16[8,144,512]{2,1,0:T(8,128)(2,1)}), bf16[8,144,512]{2,1,0:T(8,128)(2,1)S(1)}, u32[]{:S(2)}, u32[]{:S(2)}) async-start(bf16[8,144,512]{2,1,0:T(8,128)(2,1)} %bitcast.10), calls=%async_computation.3 | async-start | bytes 2359296 | tf_op jit(solution)/shard_map/all_to_all | solution.py:77
Sparse Core Ops, SparseCore 0:
  175.1 52.5 all-gather.4
  234.1 52.9 all-gather.6
where the time goes:
time: 405 us; the launch traced here: 404 us
  waiting for transfers between devices  173 us (43%)
  blocking collectives  124 us (31%)
  starting transfers between devices  62.9 us (16%)
  matrix products  16.3 us (4%)
  between operations  13.6 us (3%)
  other arithmetic  11 us (3%)
    all_to_all x1, blocking collectives, body(): lax.all_to_all(mixed.astype(jnp.bfloat16).reshape(groups, per_group, widt...  72.3 us
    all_gather x1, waiting for transfers between devices, body(): hidden = lax.all_gather(hidden, 'tp', axis=1, tiled=True)  53.1 us
    all_gather x1, waiting for transfers between devices, body(): piece = lax.all_gather(received, 'tp', axis=1, tiled=True)  52.6 us
    all_to_all x1, starting transfers between devices, body(): lax.all_to_all(facts.reshape(groups, per_group, 4), 'g', 0, 0, tiled=True)  42.5 us
    all_to_all x1, blocking collectives, body(): lax.all_to_all(buffer.reshape(members, groups * capacity, width), 'e', 0,...  40.5 us
    all_to_all x1, waiting for transfers between devices, body(): lax.all_to_all(by_group.reshape(groups, per_group, width), 'g', 0, 0, til...  34.6 us
    all_to_all x1, waiting for transfers between devices, body(): lax.all_to_all(result.reshape(members, groups * capacity, width), 'e', 0,...  25.9 us
    all_to_all x1, starting transfers between devices, body(): lax.all_to_all(by_group.reshape(groups, per_group, width), 'g', 0, 0, til...  15 us
  transfers between devices with their start and end apart: 5, of which 5 were waited for; matrix products, arithmetic and copies ran while one was open for 2% of the time, Pallas kernels for 0%

commit v1 on v0

--- a/solution.py
+++ b/solution.py
@@ -7,6 +7,13 @@
 GRP_EP = ("grp", "g", "e")
 EP = ("g", "e")
 GROUP_SIZE = 8
+
+
+def _map_state(row_data, along_axis):
+    top = jnp.stack([row_data] * lax.axis_size(along_axis), axis=0)
+    x_now = lax.all_to_all(top, along_axis, 0, 0)
+    spare = jnp.concatenate(x_now, axis=1)
+    return spare
 
 
 def rank_before(marks):
@@ -72,7 +79,7 @@
     gate = jnp.dot(piece, w_gate[0], preferred_element_type=jnp.float32)
     up = jnp.dot(piece, w_up[0], preferred_element_type=jnp.float32)
     hidden = (jax.nn.silu(gate) * up).astype(jnp.bfloat16)
-    hidden = lax.all_gather(hidden, "tp", axis=1, tiled=True)
+    hidden = _map_state(hidden, "tp")
     result = jnp.dot(hidden, w_down[0], preferred_element_type=jnp.float32).astype(jnp.bfloat16)
     back = lax.all_to_all(
         result.reshape(members, groups * capacity, width), "e", 0, 0, tiled=True

time: 405 us -> 382 us (0.943)
  waiting for transfers between devices: 173 us -> 120 us
  blocking collectives: 124 us -> 156 us
    all_gather x1 -> x0, waiting for transfers between devices: 53.1 us -> none  [body(): hidden = lax.all_gather(hidden, 'tp', axis=1, tiled=True)]
    all_to_all x0 -> x1, blocking collectives: none -> 32.2 us  [_map_state(): x_now = lax.all_to_all(top, along_axis, 0, 0)]
  transfers between devices with their start and end apart: 5 -> 4, of which waited for: 5 -> 4; matrix products, arithmetic and copies ran while one was open for 2% -> 3% of each run, Pallas kernels for 0% -> 0%
where the time goes in v1:
time: 382 us; the launch traced here: 381 us
  blocking collectives  156 us (41%)
  waiting for transfers between devices  120 us (31%)
  starting transfers between devices  62.9 us (16%)
  matrix products  13.9 us (4%)
  between operations  13.6 us (4%)
  other arithmetic  11 us (3%)
    all_to_all x1, blocking collectives, body(): lax.all_to_all(mixed.astype(jnp.bfloat16).reshape(groups, per_group, widt...  72.3 us
    all_gather x1, waiting for transfers between devices, body(): piece = lax.all_gather(received, 'tp', axis=1, tiled=True)  52.7 us
    all_to_all x1, starting transfers between devices, body(): lax.all_to_all(facts.reshape(groups, per_group, 4), 'g', 0, 0, tiled=True)  42.5 us
    all_to_all x1, blocking collectives, body(): lax.all_to_all(buffer.reshape(members, groups * capacity, width), 'e', 0,...  40.5 us
    all_to_all x1, waiting for transfers between devices, body(): lax.all_to_all(by_group.reshape(groups, per_group, width), 'g', 0, 0, til...  34.6 us
    all_to_all x1, blocking collectives, _map_state(): x_now = lax.all_to_all(top, along_axis, 0, 0)  32.2 us
    all_to_all x1, waiting for transfers between devices, body(): lax.all_to_all(result.reshape(members, groups * capacity, width), 'e', 0,...  25.9 us
    all_to_all x1, starting transfers between devices, body(): lax.all_to_all(by_group.reshape(groups, per_group, width), 'g', 0, 0, til...  15 us
  transfers between devices with their start and end apart: 4, of which 4 were waited for; matrix products, arithmetic and copies ran while one was open for 3% of the time, Pallas kernels for 0%

profile of v1, /device:TPU:96, one launch (start us, length us, event | category | flops | bytes accessed | tf_op | source)
XLA Modules:
  0.0 381.3 jit_solution(2765265813732491599)
XLA Ops:
  6.6 0.8 convert_element_type.48
  7.3 0.7 fusion.29
  8.0 0.8 reduce-window.6
  9.1 0.8 fusion.28
  9.9 0.7 multiply_add_fusion.1
  10.6 0.7 reduce_sum.57
  11.3 0.7 multiply_divide_fusion
  12.5 0.7 reshape.102
  13.2 42.5 %all-to-all-start = ((f32[8,1,192]{2,1,0:T(1,128)}), f32[8,1,192]{2,1,0:T(1,128)S(1)}, u32[]{:S(2)}, u32[]{:S(2)}) async-start(f32[8,1,192]{2,1,0:T(1,128)} %reshape.102), calls=%async_computation | async-start | bytes 16384 | tf_op jit(solution)/shard_map/all_to_all | solution.py:59
  55.7 1.2 fusion.17
  56.9 11.4 %all-gather.1 = f32[4,1,384]{2,1,0:T(1,128)S(1)} all-gather(f32[1,1,384]{2,1,0:T(1,128)S(1)} %reshape.94), channel_id=2, replica_groups=mesh['grp'=2,'g'=8,'e'=8,'tp'=4] {'tp'}, dimensions={0}, use_global_device_ids=true | all-gather | bytes 7680 | tf_op jit(solution)/shard_map/all_gather | solution.py:47
  68.3 0.8 dynamic_slice.3
  69.1 2.2 convolution_convert_fusion.3
  71.3 6.7 %all-to-all-done = f32[8,1,192]{2,1,0:T(1,128)S(1)} async-done(((f32[8,1,192]{2,1,0:T(1,128)}), f32[8,1,192]{2,1,0:T(1,128)S(1)}, u32[]{:S(2)}, u32[]{:S(2)}) %all-to-all-start) | async-done | bytes 6176 | tf_op jit(solution)/shard_map/all_to_all | solution.py:59
  78.0 15.0 %all-to-all-start.1 = ((bf16[8,48,512]{2,1,0:T(8,128)(2,1)}), bf16[8,48,512]{2,1,0:T(8,128)(2,1)S(1)}, u32[]{:S(2)}, u32[]{:S(2)}) async-start(bf16[8,48,512]{2,1,0:T(8,128)(2,1)} %bitcast.3), calls=%async_computation.1 | async-start | bytes 786432 | tf_op jit(solution)/shard_map/all_to_all | solution.py:56
  93.1 0.6 broadcast.46
  93.7 0.7 reduce.11
  94.8 3.8 reduce-window_subtract_fusion
  98.9 34.6 %all-to-all-done.1 = bf16[8,48,512]{2,1,0:T(8,128)(2,1)S(1)} async-done(((bf16[8,48,512]{2,1,0:T(8,128)(2,1)}), bf16[8,48,512]{2,1,0:T(8,128)(2,1)S(1)}, u32[]{:S(2)}, u32[]{:S(2)}) %all-to-all-start.1) | async-done | bytes 393248 | tf_op jit(solution)/shard_map/all_to_all | solution.py:56
  133.6 0.8 convolution_convert_fusion.1
  134.4 40.5 %all_to_all.30 = bf16[8,144,512]{2,1,0:T(8,128)(2,1)} all-to-all(bf16[8,144,512]{2,1,0:T(8,128)(2,1)S(1)} %bitcast.54), channel_id=1, replica_groups=mesh['grp'=2,'g'=8,'e'=8,'tp'=4] {'e'}, dimensions={0} | all-to-all | bytes 2359296 | tf_op jit(solution)/shard_map/all_to_all | solution.py:75
  175.0 52.7 %all-gather.4.cloned.1.call-done = bf16[1152,2048]{1,0:T(8,128)(2,1)} async-done(((bf16[1152,512]{1,0:T(8,128)(2,1)}), bf16[1152,2048]{1,0:T(8,128)(2,1)}) %all-gather.4.cloned.1.call-update) | async-done | bytes 4718608 | tf_op jit(solution)/shard_map/all_gather | solution.py:78
  227.7 3.9 %fusion.11 = f32[1152,256]{1,0:T(8,128)S(1)} fusion(bf16[1152,2048]{1,0:T(8,128)(2,1)} %all-gather.4.cloned.1.call-done, bf16[1,2048,256]{2,1,0:T(8,128)(2,1)S(1)} %copy-done.2), kind=kOutput, calls=%fused_computation.20 | convolution fusion | flops 1207959552 | bytes 6946816 | tf_op jit(solution)/shard_map/dot_general | solution.py:79
  231.6 1.6 fusion
  233.6 32.2 %all_to_all.31 = bf16[4,1152,256]{1,2,0:T(8,128)(2,1)S(1)} all-to-all(bf16[4,1152,256]{1,2,0:T(8,128)(2,1)S(1)} %stack.2), channel_id=1, replica_groups=mesh['grp'=2,'g'=8,'e'=8,'tp'=4] {'tp'}, dimensions={0} | all-to-all | bytes 4718592 | tf_op jit(solution)/shard_map/all_to_all | solution.py:14
  265.8 2.4 convolution_convert_fusion
  268.2 5.3 %all-to-all-start.4 = ((bf16[8,144,512]{2,1,0:T(8,128)(2,1)}), bf16[8,144,512]{2,1,0:T(8,128)(2,1)S(1)}, u32[]{:S(2)}, u32[]{:S(2)}) async-start(bf16[8,144,512]{2,1,0:T(8,128)(2,1)} %bitcast.12), calls=%async_computation.4 | async-start | bytes 2359296 | tf_op jit(solution)/shard_map/all_to_all | solution.py:84
  273.5 25.9 %all-to-all-done.4 = bf16[8,144,512]{2,1,0:T(8,128)(2,1)S(1)} async-done(((bf16[8,144,512]{2,1,0:T(8,128)(2,1)}), bf16[8,144,512]{2,1,0:T(8,128)(2,1)S(1)}, u32[]{:S(2)}, u32[]{:S(2)}) %all-to-all-start.4) | async-done | bytes 1179680 | tf_op jit(solution)/shard_map/all_to_all | solution.py:84
  299.5 0.7 fusion.7
  300.2 0.7 fusion.8
  300.9 72.3 %all_to_all.32 = bf16[8,48,512]{2,1,0:T(8,128)(2,1)S(1)} all-to-all(bf16[8,48,512]{2,1,0:T(8,128)(2,1)S(1)} %bitcast.56), channel_id=1, replica_groups=mesh['grp'=2,'g'=8,'e'=8,'tp'=4] {'g'}, dimensions={0} | all-to-all | bytes 786432 | tf_op jit(solution)/shard_map/all_to_all | solution.py:92
  373.2 1.2 convolution_convert_fusion.2
  (37 shorter events, 2.2 us)
Async XLA Ops:
  6.5 259.3 %copy-start = (bf16[1,1024,512]{2,1,0:T(8,128)(2,1)S(1)}, bf16[1,1024,512]{2,1,0:T(8,128)(2,1)}, u32[]{:S(2)}) copy-start(bf16[1,1024,512]{2,1,0:T(8,128)(2,1)} %param.17) | copy-start | bytes 3145732
  13.2 64.8 %all-to-all-start = ((f32[8,1,192]{2,1,0:T(1,128)}), f32[8,1,192]{2,1,0:T(1,128)S(1)}, u32[]{:S(2)}, u32[]{:S(2)}) async-start(f32[8,1,192]{2,1,0:T(1,128)} %reshape.102), calls=%async_computation | async-start | bytes 16384 | tf_op jit(solution)/shard_map/all_to_all | solution.py:59
  78.0 55.6 %all-to-all-start.1 = ((bf16[8,48,512]{2,1,0:T(8,128)(2,1)}), bf16[8,48,512]{2,1,0:T(8,128)(2,1)S(1)}, u32[]{:S(2)}, u32[]{:S(2)}) async-start(bf16[8,48,512]{2,1,0:T(8,128)(2,1)} %bitcast.3), calls=%async_computation.1 | async-start | bytes 786432 | tf_op jit(solution)/shard_map/all_to_all | solution.py:56
  92.9 134.7 %all-gather.4.cloned.1.call-start = ((), (), s32[]{:S(2)}) async-start(), calls=%async_computation.6 | async-start | bytes 5898240 | tf_op jit(solution)/shard_map/all_gather | solution.py:78
  174.9 52.8 %copy-start.2 = (bf16[1,2048,256]{2,1,0:T(8,128)(2,1)S(1)}, bf16[1,2048,256]{2,1,0:T(8,128)(2,1)}, u32[]{:S(2)}) copy-start(bf16[1,2048,256]{2,1,0:T(8,128)(2,1)} %param.15) | copy-start | bytes 3145732
  174.9 56.6 %copy-start.3 = (bf16[1,2048,256]{2,1,0:T(8,128)(2,1)S(1)}, bf16[1,2048,256]{2,1,0:T(8,128)(2,1)}, u32[]{:S(2)}) copy-start(bf16[1,2048,256]{2,1,0:T(8,128)(2,1)} %param.16) | copy-start | bytes 3145732
  227.7 3.9 %copy-start.1 = (bf16[1152,2048]{1,0:T(8,128)(2,1)S(1)}, bf16[1152,2048]{1,0:T(8,128)(2,1)}, u32[]{:S(2)}) copy-start(bf16[1152,2048]{1,0:T(8,128)(2,1)} %all-gather.4.cloned.1.call-done) | copy-start | bytes 14155780
  268.2 31.2 %all-to-all-start.4 = ((bf16[8,144,512]{2,1,0:T(8,128)(2,1)}), bf16[8,144,512]{2,1,0:T(8,128)(2,1)S(1)}, u32[]{:S(2)}, u32[]{:S(2)}) async-start(bf16[8,144,512]{2,1,0:T(8,128)(2,1)} %bitcast.12), calls=%async_computation.4 | async-start | bytes 2359296 | tf_op jit(solution)/shard_map/all_to_all | solution.py:84
Sparse Core Ops, SparseCore 0:
  175.1 52.5 all-gather.3
